TPU v7x, 32 devices: a whole 2x2x4 slice. The times are simulated.
32 devices in a mesh: fs: 8 (over z, y), tp: 4 (over x, core).
Axes of the slice: x: 2, y: 2, z: 4, core: 2. Of those that a mesh axis runs over, the one named last changes fastest.
Arguments:
- inputs: bfloat16 [4608, 2048], P('fs'), may hold values from -6 to 6
- query_cotangent: bfloat16 [4608, 1024], P('fs', 'tp'), may hold values from -0.017944336 to 0.017944336
- value_cotangent: bfloat16 [4608, 1024], P('fs', 'tp'), may hold values from -0.017944336 to 0.017944336
- weights_query: float32 [2048, 1024], P('fs', 'tp'), may hold values from -6 to 6
- weights_value: float32 [2048, 1024], P('fs', 'tp'), may hold values from -6 to 6
- basis_query: bfloat16 [1024, 32], P('tp'), may hold values from -0.75 to 0.75
- basis_value: bfloat16 [1024, 32], P('tp'), may hold values from -0.75 to 0.75
- first_query: float32 [2048, 512], P('fs', 'tp'), may hold values from -5.4 to 5.4, as said below
- second_query: float32 [2048, 512], P('fs', 'tp'), may hold values from 0.05 to 1
- first_value: float32 [2048, 512], P('fs', 'tp'), may hold values from -5.4 to 5.4, as said below
- second_value: float32 [2048, 512], P('fs', 'tp'), may hold values from 0.05 to 1
Outputs:
- step_query: float32 [2048, 1024], P('fs', 'tp')
- step_value: float32 [2048, 1024], P('fs', 'tp')
- new_query: float32 [2048, 1024], P('fs', 'tp')
- new_value: float32 [2048, 1024], P('fs', 'tp')
- copy_query: bfloat16 [2048, 1024], P(None, 'tp')
- copy_value: bfloat16 [2048, 1024], P(None, 'tp')
- moment_query: float32 [2048, 512], P('fs', 'tp')
- square_query: float32 [2048, 512], P('fs', 'tp')
- moment_value: float32 [2048, 512], P('fs', 'tp')
- square_value: float32 [2048, 512], P('fs', 'tp')
Inputs may be any that keep to these rules, and one draw needn't show every extreme that they name: `first_query`: first moments, with a spread of scale from row to row. `first_value`: first moments, with a spread of scale from row to row.
All inputs are finite; a program needn't handle non-finite values.
Results may differ from a plain program's by a relative error of at most 0.003.
Values may be sent and summed in bfloat16 or wider, within the bound.
A program may use at most 64 MiB of HBM per device.

v0:
```python
import jax
import jax.numpy as jnp
from jax import lax
from jax.sharding import PartitionSpec as P

D = 2048
HEADS = 16
HEAD = 64
RK = 32


def from_space(direction, factor, heads_here):
    count = direction.shape[0]
    split = direction.reshape(count, heads_here, RK)
    out = jnp.einsum("nhr,hdr->nhd", split, factor, precision=lax.Precision.HIGHEST)
    return out.reshape(count, heads_here * HEAD)


def moments(reduced, first, second):
    moment = 0.9 * first + 0.1 * reduced
    square = 0.95 * second + 0.05 * reduced * reduced
    direction = moment / (jnp.sqrt(square) + 1e-08)
    return (moment, square, direction)


def per_device(
    inputs,
    query_cotangent,
    value_cotangent,
    weights_query,
    weights_value,
    basis_query,
    basis_value,
    first_query,
    second_query,
    first_value,
    second_value,
):
    own_cols = weights_query.shape[1]
    heads_here = own_cols // HEAD
    space_cols = heads_here * RK
    factor_q = basis_query.reshape(heads_here, HEAD, RK).astype(jnp.float32)
    factor_v = basis_value.reshape(heads_here, HEAD, RK).astype(jnp.float32)
    contract = (((0,), (0,)), ((), ()))
    tok_count = query_cotangent.shape[0]
    bf_q = basis_query.reshape(heads_here, HEAD, RK)
    bf_v = basis_value.reshape(heads_here, HEAD, RK)
    small_q = jnp.einsum(
        "thd,hdr->thr",
        query_cotangent.reshape(tok_count, heads_here, HEAD),
        bf_q,
        preferred_element_type=jnp.float32,
    )
    small_v = jnp.einsum(
        "thd,hdr->thr",
        value_cotangent.reshape(tok_count, heads_here, HEAD),
        bf_v,
        preferred_element_type=jnp.float32,
    )
    small_both = jnp.concatenate(
        (small_q.reshape(tok_count, space_cols), small_v.reshape(tok_count, space_cols)), axis=1
    )
    upper_part = small_both.astype(jnp.bfloat16)
    lower_part = (small_both - upper_part.astype(jnp.float32)).astype(jnp.bfloat16)
    high = lax.dot_general(inputs, upper_part, contract, preferred_element_type=jnp.float32)
    reduced = lax.psum_scatter(
        high + lax.dot_general(inputs, lower_part, contract, preferred_element_type=jnp.float32),
        "fs",
        scatter_dimension=0,
        tiled=True,
    )
    reduced_q = reduced[:, :space_cols]
    reduced_v = reduced[:, space_cols:]
    moment_q, square_q, direction_q = moments(reduced_q, first_query, second_query)
    moment_v, square_v, direction_v = moments(reduced_v, first_value, second_value)
    total_q, total_v = lax.psum(
        (jnp.sum(direction_q * direction_q), jnp.sum(direction_v * direction_v)), ("fs", "tp")
    )
    entries = D * HEADS * RK
    scale_q = 1.0 / jnp.sqrt(total_q / entries + 0.25)
    scale_v = 1.0 / jnp.sqrt(total_v / entries + 0.25)
    step_q = scale_q * from_space(direction_q, factor_q, heads_here)
    step_v = scale_v * from_space(direction_v, factor_v, heads_here)
    fresh_q = weights_query - 0.1 * step_q
    fresh_v = weights_value - 0.1 * step_v
    copy_q, copy_v = (
        lax.all_gather(fresh_q.astype(jnp.bfloat16), "fs", axis=0, tiled=True),
        lax.all_gather(fresh_v.astype(jnp.bfloat16), "fs", axis=0, tiled=True),
    )
    return (
        step_q,
        step_v,
        fresh_q,
        fresh_v,
        copy_q,
        copy_v,
        moment_q,
        square_q,
        moment_v,
        square_v,
    )


def solution(mesh):
    placed = (
        P("fs", None),
        P("fs", "tp"),
        P("fs", "tp"),
        P("fs", "tp"),
        P("fs", "tp"),
        P("tp", None),
        P("tp", None),
        P("fs", "tp"),
        P("fs", "tp"),
        P("fs", "tp"),
        P("fs", "tp"),
    )
    return jax.shard_map(
        per_device,
        mesh=mesh,
        in_specs=placed,
        out_specs=(
            P("fs", "tp"),
            P("fs", "tp"),
            P("fs", "tp"),
            P("fs", "tp"),
            P(None, "tp"),
            P(None, "tp"),
            P("fs", "tp"),
            P("fs", "tp"),
            P("fs", "tp"),
            P("fs", "tp"),
        ),
        check_vma=False,
    )
```

profile of v0, /device:TPU:0, one launch (start us, length us, event | category | flops | bytes accessed | tf_op | source)
XLA Modules:
  0.0 223.8 jit_solution(16746739006652718097)
XLA Ops:
  7.2 1.0 reshape.52
  8.2 0.8 reshape.55
  9.0 1.2 copy.40
  10.2 1.2 copy.42
  11.4 0.2 fusion.10
  11.6 0.2 fusion.7
  11.8 1.0 fusion.2
  12.8 2.3 %fusion = f32[2048,256]{0,1:T(8,128)} fusion(f32[256,2048]{1,0:T(8,128)S(1)} %fusion.2, bf16[576,2048]{1,0:T(8,128)(2,1)S(1)} %copy-done, f32[576,128]{0,1:T(8,128)S(1)} %bitcast.31, f32[576,128]{0,1:T(8,128)S(1)} %bitcast.29), kind=kOutput, calls=%fused_computation.1 | convolution fusion | flops 605241344 | bytes 7143424 | tf_op jit(solution)/shard_map/dot_general | solution.py:67
  15.3 0.7 copy-done.6
  16.4 70.6 %reduce-scatter.2.cloned.1.call-done = f32[256,256]{0,1:T(8,128)} async-done(((f32[2048,256]{0,1:T(8,128)}), f32[256,256]{0,1:T(8,128)}) %reduce-scatter.2.cloned.1.call-update) | async-done | bytes 262160 | tf_op jit(solution)/shard_map/reduce_scatter | solution.py:66
  86.9 2.4 %multiply_reduce_fusion = (f32[]{:T(128)}, f32[256,128]{0,1:T(8,128)S(1)}, f32[256,128]{0,1:T(8,128)}, f32[256,128]{0,1:T(8,128)S(1)}, f32[]{:T(128)}, /*index=5...) fusion(f32[256,256]{0,1:T(8,128)} %reduce-scatter.2.cloned.1.call-done, f32[256,128]{0,1:T(8,128)S(1)} %copy.47, ...), kind=kLoop, calls=%fused_computation.14 | loop fusion | flops 720894 | bytes 1572872 | tf_op jit(solution)/shard_map/reduce_sum | solution.py:77
  89.3 39.8 %all-reduce = (f32[]{:T(128)}, f32[]{:T(128)}) all-reduce(f32[]{:T(128)} %get-tuple-element.44, f32[]{:T(128)} %get-tuple-element.36), channel_id=1, replica_groups=mesh['fs'=8,'tp'=4] {'fs','tp'}, use_global_device_ids=true, to_apply=%region_2.0 | all-reduce | flops 2 | bytes 16 | tf_op jit(solution)/shard_map/psum | solution.py:76
  129.8 0.3 convolution_multiply_fusion
  130.3 1.8 fusion.14
  132.9 1.2 convolution_multiply_fusion.1
  134.2 1.8 fusion.15
  136.1 1.7 copy.56
  137.8 0.8 copy.55
  138.5 0.8 copy.54
  139.3 0.8 copy.53
  140.0 32.2 %all-gather.5.cloned.1.call-done = bf16[2048,256]{1,0:T(8,128)(2,1)} async-done(((bf16[256,256]{1,0:T(8,128)(2,1)}), bf16[2048,256]{1,0:T(8,128)(2,1)}) %all-gather.5.cloned.1.call-update) | async-done | bytes 1048592 | tf_op jit(solution)/shard_map/all_gather | solution.py:88
  172.3 41.7 %all-gather.3.cloned.1.call-done = bf16[2048,256]{1,0:T(8,128)(2,1)} async-done(((bf16[256,256]{1,0:T(8,128)(2,1)}), bf16[2048,256]{1,0:T(8,128)(2,1)}) %all-gather.3.cloned.1.call-update) | async-done | bytes 1048592 | tf_op jit(solution)/shard_map/all_gather | solution.py:87
  214.0 2.4 %copy.67 = bf16[2048,256]{1,0:T(8,128)(2,1)} copy(bf16[2048,256]{1,0:T(8,128)(2,1)} %all-gather.3.cloned.1.call-done) | data formatting | bytes 2097152
  216.3 1.0 copy.68
  (29 shorter events, 0.9 us)
Async XLA Ops:
  7.2 4.6 %copy-start = (bf16[576,2048]{1,0:T(8,128)(2,1)S(1)}, bf16[576,2048]{1,0:T(8,128)(2,1)}, u32[]{:S(2)}) copy-start(bf16[576,2048]{1,0:T(8,128)(2,1)} %param.11) | copy-start | bytes 7077892
  7.2 79.7 %reduce-scatter.2.cloned.1.call-start = ((), (), s32[]{:S(2)}) async-start(), calls=%async_computation.1 | async-start | bytes 2359296 | tf_op jit(solution)/shard_map/reduce_scatter | solution.py:66
  8.2 4.6 %copy-start.4 = (bf16[4,64,32]{1,0,2:T(4,128)(2,1)}, bf16[4,64,32]{1,0,2:T(4,128)(2,1)S(1)}, u32[]{:S(2)}) copy-start(bf16[4,64,32]{1,0,2:T(4,128)(2,1)S(1)} %reshape.52) | copy-start | bytes 49156
  12.8 2.4 %copy-start.5 = (f32[256,128]{1,0:T(8,128)S(1)}, f32[256,128]{1,0:T(8,128)}, u32[]{:S(2)}) copy-start(f32[256,128]{1,0:T(8,128)} %param.18) | copy-start | bytes 393220
  15.1 0.9 copy-start.6
  15.1 1.0 copy-start.7
  15.1 1.1 copy-start.8
  15.2 157.1 %all-gather.5.cloned.1.call-start = ((), (), s32[]{:S(2)}) async-start(), calls=%async_computation.3 | async-start | bytes 1179648 | tf_op jit(solution)/shard_map/all_gather | solution.py:88
  130.3 86.1 %copy-start.1 = (f32[256,256]{1,0:T(8,128)}, f32[256,256]{1,0:T(8,128)S(1)}, u32[]{:S(2)}) copy-start(f32[256,256]{1,0:T(8,128)S(1)} %copy.52) | copy-start | bytes 786436
  132.1 81.8 %all-gather.3.cloned.1.call-start = ((), (), s32[]{:S(2)}) async-start(), calls=%async_computation.2 | async-start | bytes 1179648 | tf_op jit(solution)/shard_map/all_gather | solution.py:87
  134.2 83.1 %copy-start.2 = (f32[256,256]{1,0:T(8,128)}, f32[256,256]{1,0:T(8,128)S(1)}, u32[]{:S(2)}) copy-start(f32[256,256]{1,0:T(8,128)S(1)} %copy.51) | copy-start | bytes 786436
  214.0 2.4 %copy-start.3 = (bf16[2048,256]{1,0:T(8,128)(2,1)S(1)}, bf16[2048,256]{1,0:T(8,128)(2,1)}, u32[]{:S(2)}) copy-start(bf16[2048,256]{1,0:T(8,128)(2,1)} %all-gather.5.cloned.1.call-done) | copy-start | bytes 3145732
Sparse Core Ops, SparseCore 0:
  15.3 71.6 reduce-scatter.1
  132.3 39.9 all-gather.4
  175.0 38.9 all-gather.2
where the time goes:
time: 224 us
  waiting for transfers between devices  145 us (65%)
  blocking collectives  39.8 us (18%)
  between operations  15.3 us (7%)
  local copies, waits for them, and re-layouts  12.7 us (6%)
  other arithmetic  6.06 us (3%)
  matrix products  5.25 us (2%)
    reduce_scatter x1, waiting for transfers between devices, per_device(): lax.psum_scatter(high + lax.dot_general(inputs, lower_part, contract, pre...  70.6 us
    all_gather x1, waiting for transfers between devices, per_device(): lax.all_gather(fresh_q.astype(jnp.bfloat16), 'fs', axis=0, tiled=True)  41.7 us
    psum x1, blocking collectives, per_device(): lax.psum((jnp.sum(direction_q * direction_q), jnp.sum(direction_v * direc...  39.8 us
    all_gather x1, waiting for transfers between devices, per_device(): lax.all_gather(fresh_v.astype(jnp.bfloat16), 'fs', axis=0, tiled=True)  32.2 us
    unnamed x32, local copies, waits for them, and re-layouts  11 us
  transfers between devices with their start and end apart: 3, of which 3 were waited for; matrix products, arithmetic and copies ran while one was open for 3% of the time, Pallas kernels for 0%

commit v1 on v0

--- a/solution.py
+++ b/solution.py
@@ -7,6 +7,11 @@
 HEADS = 16
 HEAD = 64
 RK = 32
+
+
+def axis_by_axis(value, one, other):
+    half = lax.psum(value, one)
+    return lax.psum(half, other)
 
 
 def from_space(direction, factor, heads_here):
@@ -73,8 +78,8 @@
     reduced_v = reduced[:, space_cols:]
     moment_q, square_q, direction_q = moments(reduced_q, first_query, second_query)
     moment_v, square_v, direction_v = moments(reduced_v, first_value, second_value)
-    total_q, total_v = lax.psum(
-        (jnp.sum(direction_q * direction_q), jnp.sum(direction_v * direction_v)), ("fs", "tp")
+    total_q, total_v = axis_by_axis(
+        (jnp.sum(direction_q * direction_q), jnp.sum(direction_v * direction_v)), "tp", "fs"
     )
     entries = D * HEADS * RK
     scale_q = 1.0 / jnp.sqrt(total_q / entries + 0.25)

time: 224 us -> 208 us (0.929)
  blocking collectives: 39.8 us -> 26 us
  waiting for transfers between devices: 145 us -> 142 us
    psum x1 -> x2, blocking collectives: 39.8 us -> 26 us  [the longest x1 19.7 us: axis_by_axis(): return lax.psum(half, other)]
  transfers between devices with their start and end apart: 3 -> 3, of which waited for: 3 -> 3; matrix products, arithmetic and copies ran while one was open for 3% -> 4% of each run, Pallas kernels for 0% -> 0%
where the time goes in v1:
time: 208 us
  waiting for transfers between devices  142 us (68%)
  blocking collectives  26 us (12%)
  between operations  15.3 us (7%)
  local copies, waits for them, and re-layouts  12.7 us (6%)
  other arithmetic  6.06 us (3%)
  matrix products  5.26 us (3%)
    reduce_scatter x1, waiting for transfers between devices, per_device(): lax.psum_scatter(high + lax.dot_general(inputs, lower_part, contract, pre...  70.6 us
    all_gather x1, waiting for transfers between devices, per_device(): lax.all_gather(fresh_q.astype(jnp.bfloat16), 'fs', axis=0, tiled=True)  41.7 us
    all_gather x1, waiting for transfers between devices, per_device(): lax.all_gather(fresh_v.astype(jnp.bfloat16), 'fs', axis=0, tiled=True)  30 us
    psum x1, blocking collectives, axis_by_axis(): return lax.psum(half, other)  19.7 us
    unnamed x32, local copies, waits for them, and re-layouts  11 us
    psum x1, blocking collectives, axis_by_axis(): half = lax.psum(value, one)  6.27 us
  transfers between devices with their start and end apart: 3, of which 3 were waited for; matrix products, arithmetic and copies ran while one was open for 4% of the time, Pallas kernels for 0%

profile of v1, /device:TPU:0, one launch (start us, length us, event | category | flops | bytes accessed | tf_op | source)
XLA Modules:
  0.0 207.9 jit_solution(15692261895530256214)
XLA Ops:
  7.2 1.0 reshape.52
  8.2 0.8 reshape.55
  9.0 1.2 copy.40
  10.2 1.2 copy.42
  11.4 0.2 fusion.10
  11.8 1.0 fusion.2
  12.8 2.4 %fusion = f32[2048,256]{0,1:T(8,128)} fusion(f32[256,2048]{1,0:T(8,128)S(1)} %fusion.2, bf16[576,2048]{1,0:T(8,128)(2,1)S(1)} %copy-done, f32[576,128]{0,1:T(8,128)S(1)} %bitcast.31, f32[576,128]{0,1:T(8,128)S(1)} %bitcast.29), kind=kOutput, calls=%fused_computation.1 | convolution fusion | flops 605241344 | bytes 7143424 | tf_op jit(solution)/shard_map/dot_general | solution.py:72
  15.3 0.7 copy-done.6
  16.4 70.6 %reduce-scatter.2.cloned.1.call-done = f32[256,256]{0,1:T(8,128)} async-done(((f32[2048,256]{0,1:T(8,128)}), f32[256,256]{0,1:T(8,128)}) %reduce-scatter.2.cloned.1.call-update) | async-done | bytes 262160 | tf_op jit(solution)/shard_map/reduce_scatter | solution.py:71
  86.9 2.4 %multiply_reduce_fusion = (f32[]{:T(128)}, f32[256,128]{0,1:T(8,128)S(1)}, f32[256,128]{0,1:T(8,128)}, f32[256,128]{0,1:T(8,128)S(1)}, f32[]{:T(128)}, /*index=5...) fusion(f32[256,256]{0,1:T(8,128)} %reduce-scatter.2.cloned.1.call-done, f32[256,128]{0,1:T(8,128)S(1)} %copy.47, ...), kind=kLoop, calls=%fused_computation.14 | loop fusion | flops 720894 | bytes 1572872 | tf_op jit(solution)/shard_map/reduce_sum | solution.py:82
  89.4 6.3 %all-reduce.1 = (f32[]{:T(128)}, f32[]{:T(128)}) all-reduce(f32[]{:T(128)} %get-tuple-element.46, f32[]{:T(128)} %get-tuple-element.38), channel_id=1, replica_groups=mesh['fs'=8,'tp'=4] {'tp'}, use_global_device_ids=true, to_apply=%region_2.0 | all-reduce | flops 2 | bytes 16 | tf_op jit(solution)/shard_map/psum | solution.py:13
  95.6 19.7 %all-reduce = (f32[]{:T(128)}, f32[]{:T(128)}) all-reduce(f32[]{:T(128)} %get-tuple-element.32, f32[]{:T(128)} %get-tuple-element.33), channel_id=1, replica_groups=mesh['fs'=8,'tp'=4] {'fs'}, use_global_device_ids=true, to_apply=%region_3.0 | all-reduce | flops 2 | bytes 16 | tf_op jit(solution)/shard_map/psum | solution.py:14
  116.0 0.3 convolution_multiply_fusion
  116.5 1.8 fusion.14
  119.1 1.2 convolution_multiply_fusion.1
  120.5 1.8 fusion.15
  122.3 1.7 copy.56
  124.0 0.8 copy.55
  124.7 0.8 copy.54
  125.5 0.8 copy.53
  126.2 30.0 %all-gather.5.cloned.1.call-done = bf16[2048,256]{1,0:T(8,128)(2,1)} async-done(((bf16[256,256]{1,0:T(8,128)(2,1)}), bf16[2048,256]{1,0:T(8,128)(2,1)}) %all-gather.5.cloned.1.call-update) | async-done | bytes 1048592 | tf_op jit(solution)/shard_map/all_gather | solution.py:93
  156.3 41.7 %all-gather.3.cloned.1.call-done = bf16[2048,256]{1,0:T(8,128)(2,1)} async-done(((bf16[256,256]{1,0:T(8,128)(2,1)}), bf16[2048,256]{1,0:T(8,128)(2,1)}) %all-gather.3.cloned.1.call-update) | async-done | bytes 1048592 | tf_op jit(solution)/shard_map/all_gather | solution.py:92
  198.0 2.4 %copy.67 = bf16[2048,256]{1,0:T(8,128)(2,1)} copy(bf16[2048,256]{1,0:T(8,128)(2,1)} %all-gather.3.cloned.1.call-done) | data formatting | bytes 2097152
  200.4 1.0 copy.68
  (30 shorter events, 1.0 us)
Async XLA Ops:
  7.2 4.6 %copy-start = (bf16[576,2048]{1,0:T(8,128)(2,1)S(1)}, bf16[576,2048]{1,0:T(8,128)(2,1)}, u32[]{:S(2)}) copy-start(bf16[576,2048]{1,0:T(8,128)(2,1)} %param.11) | copy-start | bytes 7077892
  7.2 79.8 %reduce-scatter.2.cloned.1.call-start = ((), (), s32[]{:S(2)}) async-start(), calls=%async_computation.1 | async-start | bytes 2359296 | tf_op jit(solution)/shard_map/reduce_scatter | solution.py:71
  8.2 4.6 %copy-start.4 = (bf16[4,64,32]{1,0,2:T(4,128)(2,1)}, bf16[4,64,32]{1,0,2:T(4,128)(2,1)S(1)}, u32[]{:S(2)}) copy-start(bf16[4,64,32]{1,0,2:T(4,128)(2,1)S(1)} %reshape.52) | copy-start | bytes 49156
  12.8 2.4 %copy-start.5 = (f32[256,128]{1,0:T(8,128)S(1)}, f32[256,128]{1,0:T(8,128)}, u32[]{:S(2)}) copy-start(f32[256,128]{1,0:T(8,128)} %param.18) | copy-start | bytes 393220
  15.1 0.9 copy-start.6
  15.1 1.0 copy-start.7
  15.1 1.1 copy-start.8
  15.2 141.1 %all-gather.5.cloned.1.call-start = ((), (), s32[]{:S(2)}) async-start(), calls=%async_computation.3 | async-start | bytes 1179648 | tf_op jit(solution)/shard_map/all_gather | solution.py:93
  116.5 83.9 %copy-start.1 = (f32[256,256]{1,0:T(8,128)}, f32[256,256]{1,0:T(8,128)S(1)}, u32[]{:S(2)}) copy-start(f32[256,256]{1,0:T(8,128)S(1)} %copy.52) | copy-start | bytes 786436
  118.4 79.7 %all-gather.3.cloned.1.call-start = ((), (), s32[]{:S(2)}) async-start(), calls=%async_computation.2 | async-start | bytes 1179648 | tf_op jit(solution)/shard_map/all_gather | solution.py:92
  120.5 80.9 %copy-start.2 = (f32[256,256]{1,0:T(8,128)}, f32[256,256]{1,0:T(8,128)S(1)}, u32[]{:S(2)}) copy-start(f32[256,256]{1,0:T(8,128)S(1)} %copy.51) | copy-start | bytes 786436
  198.0 2.4 %copy-start.3 = (bf16[2048,256]{1,0:T(8,128)(2,1)S(1)}, bf16[2048,256]{1,0:T(8,128)(2,1)}, u32[]{:S(2)}) copy-start(bf16[2048,256]{1,0:T(8,128)(2,1)} %all-gather.5.cloned.1.call-done) | copy-start | bytes 3145732
Sparse Core Ops, SparseCore 0:
  15.3 71.6 reduce-scatter.1
  118.5 37.7 all-gather.4
  159.0 38.9 all-gather.2
